TPU v7x, 32 devices: a whole 2x2x4 slice. The times are simulated.
32 devices in a mesh: grp: 2 (over y), kv: 4 (over z), tp: 4 (over x, core).
Axes of the slice: x: 2, y: 2, z: 4, core: 2. Of those that a mesh axis runs over, the one named last changes fastest.
Arguments:
- tokens: bfloat16 [48, 4096], P('grp', ('kv', 'tp')), parts along dimension 0, may hold values from -12 to 12
- lengths: int32 [48], P('grp'), parts along dimension 0, may hold values from 1 to 128, 1536 in all
- attn_gain: float32 [4096], P('kv'), may hold values from 0.1 to 1.9
- w_query: bfloat16 [4096, 4096], P('kv', 'tp'), may hold values from -0.09375 to 0.09375
- w_key: bfloat16 [4096, 4096], P('kv', 'tp'), may hold values from -0.09375 to 0.09375
- w_value: bfloat16 [4096, 4096], P('kv', 'tp'), may hold values from -0.09375 to 0.09375
- w_gate: bfloat16 [4096, 4096], P('kv', 'tp'), may hold values from -0.09375 to 0.09375
- log_decay: float32 [16], P('tp'), may hold values from -1 to 0
- key_cache: bfloat16 [48, 128, 4096], P('grp', 'kv', 'tp'), parts along dimension 0, may hold values from -6 to 6
- value_cache: bfloat16 [48, 128, 4096], P('grp', 'kv', 'tp'), parts along dimension 0, may hold values from -6 to 6
- gn_gain: float32 [4096], P('tp'), may hold values from 0.1 to 1.9
- w_out: bfloat16 [4096, 4096], P('tp', 'kv'), may hold values from -0.1875 to 0.1875
- ffn_gain: float32 [4096], P('kv'), may hold values from 0.1 to 1.9
- w_ffn_gate: bfloat16 [4096, 11264], P('kv', 'tp'), may hold values from -0.09375 to 0.09375
- w_ffn_up: bfloat16 [4096, 11264], P('kv', 'tp'), may hold values from -0.09375 to 0.09375
- w_ffn_down: bfloat16 [11264, 4096], P('tp', 'kv'), may hold values from -0.109375 to 0.109375
Outputs:
- layer_out: bfloat16 [48, 4096], P('grp', ('kv', 'tp')), parts along dimension 0
There are 2 independent parts, one for each index of `grp`. A program takes and returns all parts, laid end to end along the dimension named above; an argument that names none is the same for every part. Nothing has to cross between parts.
All inputs are finite; a program needn't handle non-finite values.
Results may differ from a plain program's by a relative error of at most 0.012.
Values may be sent and summed in bfloat16 or wider, within the bound.
A program may use at most 64 MiB of HBM per device.

v0:
```python
import jax
import jax.numpy as jnp
from jax import lax
from jax.sharding import PartitionSpec as P

DK = 256
D = 4096


RMS_EPS = 0.1
GN_EPS = 1.0
ROPE_BASE = 10000.0


def rotate(vectors, positions):
    half_dim = vectors.shape[-1] // 2
    inverse = ROPE_BASE ** (-jnp.arange(half_dim, dtype=jnp.float32) / half_dim)
    angles = positions[:, None, None] * inverse[None, None, :]
    cosine = jnp.cos(angles)
    sine_part = jnp.sin(angles)
    front_part = vectors[..., :half_dim]
    back_part = vectors[..., half_dim:]
    return jnp.concatenate(
        [front_part * cosine - back_part * sine_part, front_part * sine_part + back_part * cosine],
        axis=-1,
    )


def group_norm(totals, gn_gain):
    width = totals.shape[-1]
    center = jnp.sum(totals, axis=-1, keepdims=True) / width
    spread = jnp.sum(totals * totals, axis=-1, keepdims=True) / width - center * center
    normed = (totals - center) * lax.rsqrt(spread + GN_EPS)
    return normed.reshape(normed.shape[0], -1) * gn_gain


def channel_stat(own_squares):
    return lax.psum(own_squares, "kv")


def input_stat(own_squares):
    return lax.psum(own_squares, "kv")


def cache_partial(query_low, lengths, log_decay, key_cache, value_cache, heads_here):
    batch_rows = query_low.shape[0]
    span = key_cache.shape[1]
    slots = lax.axis_index("kv") * span + jnp.arange(span, dtype=jnp.int32)
    live = slots[None, :] < lengths[:, None]
    gaps = jnp.maximum((lengths[:, None] - slots[None, :]).astype(jnp.float32), 0.0)
    decays = jnp.exp(log_decay[None, None, :] * gaps[:, :, None])
    keys_here = key_cache.reshape(batch_rows, span, heads_here, DK)
    values_here = value_cache.reshape(batch_rows, span, heads_here, DK)
    scores = jnp.einsum("bphd,bhd->bph", keys_here, query_low, preferred_element_type=jnp.float32)
    mixing = jnp.where(live[:, :, None], scores * decays, 0.0).astype(jnp.bfloat16)
    return jnp.einsum("bph,bphd->bhd", mixing, values_here, preferred_element_type=jnp.float32)


def local(
    tokens,
    lengths,
    attn_gain,
    w_query,
    w_key,
    w_value,
    w_gate,
    log_decay,
    key_cache,
    value_cache,
    gn_gain,
    w_out,
    ffn_gain,
    w_ffn_gate,
    w_ffn_up,
    w_ffn_down,
):
    batch_rows = tokens.shape[0]
    heads_here = log_decay.shape[0]
    row_block = lax.all_gather(tokens, "tp", axis=1, tiled=True)
    widened = row_block.astype(jnp.float32)
    own_squares = jnp.sum(widened * widened, axis=1)
    scaled = (widened * attn_gain).astype(jnp.bfloat16)
    part_query = jnp.dot(scaled, w_query, preferred_element_type=jnp.float32)
    part_key = jnp.dot(scaled, w_key, preferred_element_type=jnp.float32)
    part_value = jnp.dot(scaled, w_value, preferred_element_type=jnp.float32)
    part_gate = jnp.dot(scaled, w_gate, preferred_element_type=jnp.float32)
    positions = lengths.astype(jnp.float32)
    total_squares = input_stat(own_squares)
    queries, new_keys, new_values, gates = lax.psum(
        (part_query, part_key, part_value, part_gate), "kv"
    )
    factor = lax.rsqrt(total_squares / D + RMS_EPS)[:, None]
    queries = rotate((queries * factor).reshape(batch_rows, heads_here, DK), positions) * DK ** (
        -0.5
    )
    new_keys = rotate((new_keys * factor).reshape(batch_rows, heads_here, DK), positions)
    new_values = (new_values * factor).reshape(batch_rows, heads_here, DK)
    gates = gates * factor
    query_low = queries.astype(jnp.bfloat16)
    partial_value = cache_partial(query_low, lengths, log_decay, key_cache, value_cache, heads_here)
    cached = lax.psum(partial_value.reshape(batch_rows, heads_here * DK), "kv")
    own_term = jnp.sum(queries * new_keys, axis=-1, keepdims=True) * new_values
    normed = group_norm(cached.reshape(batch_rows, heads_here, DK) + own_term, gn_gain)
    gated = (jax.nn.silu(gates) * normed).astype(jnp.bfloat16)
    out_partial = jnp.dot(gated, w_out, preferred_element_type=jnp.float32)
    mixed = lax.psum_scatter(out_partial, "tp", scatter_dimension=1, tiled=True)
    resid = (tokens.astype(jnp.float32) + mixed).astype(jnp.bfloat16)
    resid_block = lax.all_gather(resid, "tp", axis=1, tiled=True).astype(jnp.float32)
    mid_squares = jnp.sum(resid_block * resid_block, axis=1)
    scaled_mid = (resid_block * ffn_gain).astype(jnp.bfloat16)
    gate_part = jnp.dot(scaled_mid, w_ffn_gate, preferred_element_type=jnp.float32)
    up_part = jnp.dot(scaled_mid, w_ffn_up, preferred_element_type=jnp.float32)
    total_mid = channel_stat(mid_squares)
    gate_sum, up_sum = lax.psum((gate_part, up_part), "kv")
    factor_mid = lax.rsqrt(total_mid / D + RMS_EPS)[:, None]
    hidden = (jax.nn.silu(gate_sum * factor_mid) * (up_sum * factor_mid)).astype(jnp.bfloat16)
    down_partial = jnp.dot(hidden, w_ffn_down, preferred_element_type=jnp.float32)
    down = lax.psum_scatter(down_partial, "tp", scatter_dimension=1, tiled=True)
    return (resid.astype(jnp.float32) + down).astype(jnp.bfloat16)


def solution(mesh):
    return jax.shard_map(
        local,
        mesh=mesh,
        in_specs=(
            P("grp", ("kv", "tp")),
            P("grp"),
            P("kv"),
            P("kv", "tp"),
            P("kv", "tp"),
            P("kv", "tp"),
            P("kv", "tp"),
            P("tp"),
            P("grp", "kv", "tp"),
            P("grp", "kv", "tp"),
            P("tp"),
            P("tp", "kv"),
            P("kv"),
            P("kv", "tp"),
            P("kv", "tp"),
            P("tp", "kv"),
        ),
        out_specs=P("grp", ("kv", "tp")),
        check_vma=False,
    )
```

profile of v0, /device:TPU:0, one launch (start us, length us, event | category | flops | bytes accessed | tf_op | source)
XLA Modules:
  0.0 205.3 jit_solution(9403669641854922078)
XLA Ops:
  6.5 6.6 %all_gather.6 = bf16[24,1024]{1,0:T(8,128)(2,1)S(1)} all-gather(bf16[24,256]{1,0:T(8,128)(2,1)} %param.16), channel_id=1, replica_groups=mesh['grp'=2,'kv'=4,'tp'=4] {'tp'}, dimensions={1}, use_global_device_ids=true | all-gather | bytes 61440 | tf_op jit(solution)/shard_map/all_gather | solution.py:79
  13.1 1.7 fusion.32
  15.2 12.4 %psum.64 = f32[24]{0:T(128)S(1)} all-reduce(f32[24]{0:T(128)S(1)} %fusion.13), channel_id=1, replica_groups=mesh['grp'=2,'kv'=4,'tp'=4] {'kv'}, use_global_device_ids=true, to_apply=%region_2.0 | all-reduce | flops 24 | bytes 192 | tf_op jit(solution)/shard_map/psum | solution.py:42
  27.7 2.8 %fusion.30 = f32[24,1024]{1,0:T(8,128)} fusion(bf16[1024,1024]{1,0:T(8,128)(2,1)} %param.20, bf16[24,1024]{1,0:T(8,128)(2,1)S(1)} %all_gather.6, f32[1024]{0:T(1024)S(1)} %copy-done.6), kind=kOutput, calls=%fused_computation.45 | convolution fusion | flops 50405376 | bytes 2248704 | tf_op jit(solution)/shard_map/dot_general | solution.py:84
  30.5 1.0 fusion.28
  31.5 1.0 fusion.34
  32.6 18.7 %all-reduce.6.cloned.1.call-done = f32[24,1024]{1,0:T(8,128)} async-done(((f32[24,1024]{1,0:T(8,128)}), f32[24,1024]{1,0:T(8,128)}) %all-reduce.6.cloned.1.call-update) | async-done | bytes 98320 | tf_op jit(solution)/shard_map/psum | solution.py:89
  51.3 1.0 broadcast_multiply_fusion.2
  52.4 1.9 fusion.3
  55.2 1.8 fusion
  57.7 36.8 %all-reduce.10.cloned.1.call-done = (f32[24,1024]{1,0:T(8,128)}, f32[24,1024]{1,0:T(8,128)}, f32[24,1024]{1,0:T(8,128)}, f32[24,1024]{1,0:T(8,128)}) async-done(((f32[24,1024]{1,0:T(8,128)}, f32[24,1024]{1,0:T(8,128)}, f32[24,1024]{1,0:T(8,128)}, f32[24,1024]{1,0:T(8,128)}), (f32[24,1024]{1,0:T(8,128)}, f32[24,1024]{1,0:T(8,128)}, f32[24,1024]{1,0:T(8,128)}, ...) | async-done | bytes 393232 | tf_op jit(solution)/shard_map/psum | solution.py:101
  94.6 1.0 reshape.175
  95.6 1.0 broadcast_multiply_fusion.1
  97.5 2.7 %fusion.20 = f32[24,1024]{1,0:T(8,128)} fusion(bf16[1024,1024]{1,0:T(8,128)(2,1)} %param.27, f32[24,1024]{1,0:T(8,128)S(1)} %bitcast.43, f32[24,1024]{1,0:T(8,128)S(1)} %bitcast.42, f32[24,1024]{1,0:T(8,128)S(1)} %copy-done.3, f32[24,1024]{1,0:T(8,128)S(1)} %bitcast.41, f32[24,1024]{1,0:T(8,128)S(1)} %copy-done.5, f32[1024]{0:T(1024)S(1)} %copy-done.9, ...), kind=kOutput, calls=%fused_computation.31 | convolution fusion | flops 50651136 | bytes 2789472 | tf_op jit(solution)/shard_map/dot_general | solution.py:105
  100.3 19.6 %reduce-scatter.3.cloned.1.call-done = f32[24,256]{1,0:T(8,128)} async-done(((f32[24,1024]{1,0:T(8,128)}), f32[24,256]{1,0:T(8,128)}) %reduce-scatter.3.cloned.1.call-update) | async-done | bytes 24592 | tf_op jit(solution)/shard_map/reduce_scatter | solution.py:106
  119.8 0.7 add_convert_fusion.1
  120.6 5.2 %all_gather.7 = bf16[24,1024]{1,0:T(8,128)(2,1)S(1)} all-gather(bf16[24,256]{1,0:T(8,128)(2,1)S(1)} %add_convert_fusion.1), channel_id=1, replica_groups=mesh['grp'=2,'kv'=4,'tp'=4] {'tp'}, dimensions={1}, use_global_device_ids=true | all-gather | bytes 61440 | tf_op jit(solution)/shard_map/all_gather | solution.py:108
  125.8 4.2 %fusion.24 = f32[24,2816]{1,0:T(8,128)} fusion(bf16[1024,2816]{1,0:T(8,128)(2,1)} %param.30, bf16[24,1024]{1,0:T(8,128)(2,1)S(1)} %all_gather.7, f32[1024]{0:T(1024)S(1)} %copy-done.8), kind=kOutput, calls=%fused_computation.42 | convolution fusion | flops 138485760 | bytes 6090752 | tf_op jit(solution)/shard_map/dot_general | solution.py:112
  130.0 4.2 %fusion.26 = f32[24,2816]{1,0:T(8,128)} fusion(bf16[1024,2816]{1,0:T(8,128)(2,1)} %param.29, bf16[24,1024]{1,0:T(8,128)(2,1)S(1)} %all_gather.7, f32[1024]{0:T(1024)S(1)} %copy-done.8), kind=kOutput, calls=%fused_computation.43 | convolution fusion | flops 138485760 | bytes 6090752 | tf_op jit(solution)/shard_map/dot_general | solution.py:111
  134.4 11.9 %psum.70 = f32[24]{0:T(128)S(1)} all-reduce(f32[24]{0:T(128)S(1)} %fusion.15), channel_id=1, replica_groups=mesh['grp'=2,'kv'=4,'tp'=4] {'kv'}, use_global_device_ids=true, to_apply=%region_13.14 | all-reduce | flops 24 | bytes 192 | tf_op jit(solution)/shard_map/psum | solution.py:38
  146.3 26.8 %all-reduce.8.cloned.1.call-done = (f32[24,2816]{1,0:T(8,128)}, f32[24,2816]{1,0:T(8,128)}) async-done(((f32[24,2816]{1,0:T(8,128)}, f32[24,2816]{1,0:T(8,128)}), (f32[24,2816]{1,0:T(8,128)}, f32[24,2816]{1,0:T(8,128)})) %all-reduce.8.cloned.1.call-update) | async-done | bytes 540688 | tf_op jit(solution)/shard_map/psum | solution.py:114
  173.1 4.4 %fusion.9 = f32[24,1024]{1,0:T(8,128)} fusion(bf16[2816,1024]{1,0:T(8,128)(2,1)} %param.31, f32[24,2816]{1,0:T(8,128)} %get-tuple-element.7, f32[24,2816]{1,0:T(8,128)} %get-tuple-element.8, f32[24]{0:T(128)S(1)} %add_rsqrt_fusion.1), kind=kOutput, calls=%fused_computation.11 | convolution fusion | flops 138952704 | bytes 6406240 | tf_op jit(solution)/shard_map/dot_general | solution.py:117
  177.5 19.9 %reduce-scatter.5.cloned.1.call-done = f32[24,256]{1,0:T(8,128)} async-done(((f32[24,1024]{1,0:T(8,128)}), f32[24,256]{1,0:T(8,128)}) %reduce-scatter.5.cloned.1.call-update) | async-done | bytes 24592 | tf_op jit(solution)/shard_map/reduce_scatter | solution.py:118
  197.4 1.3 add_convert_fusion
  (64 shorter events, 3.2 us)
Async XLA Ops:
  6.5 6.6 %copy-start = (bf16[1024,1024]{1,0:T(8,128)(2,1)S(1)}, bf16[1024,1024]{1,0:T(8,128)(2,1)}, u32[]{:S(2)}) copy-start(bf16[1024,1024]{1,0:T(8,128)(2,1)} %param.19) | copy-start | bytes 6291460
  6.5 21.1 %copy-start.6 = (f32[1024]{0:T(1024)S(1)}, f32[1024]{0:T(1024)}, u32[]{:S(2)}) copy-start(f32[1024]{0:T(1024)} %param.18) | copy-start | bytes 12292
  6.5 8.4 %copy-start.10 = (s32[24]{0:T(128)S(1)}, s32[24]{0:T(128)}, u32[]{:S(2)}) copy-start(s32[24]{0:T(128)} %param.17) | copy-start | bytes 292
  6.5 44.8 %all-reduce.6.cloned.1.call-start = ((), (), s32[]{:S(2)}) async-start(), calls=%async_computation.2 | async-start | bytes 196608 | tf_op jit(solution)/shard_map/psum | solution.py:89
  14.9 79.7 %all-reduce.10.cloned.1.call-start = ((), (), s32[]{:S(2)}) async-start(), calls=%async_computation.6 | async-start | bytes 786432 | tf_op jit(solution)/shard_map/psum | solution.py:101
  27.7 2.8 %copy-start.1 = (bf16[1024,1024]{1,0:T(8,128)(2,1)S(1)}, bf16[1024,1024]{1,0:T(8,128)(2,1)}, u32[]{:S(2)}) copy-start(bf16[1024,1024]{1,0:T(8,128)(2,1)} %param.21) | copy-start | bytes 6291460
  27.7 3.8 %copy-start.2 = (bf16[1024,1024]{1,0:T(8,128)(2,1)S(1)}, bf16[1024,1024]{1,0:T(8,128)(2,1)}, u32[]{:S(2)}) copy-start(bf16[1024,1024]{1,0:T(8,128)(2,1)} %param.22) | copy-start | bytes 6291460
  32.5 22.1 %copy-start.11 = (f32[4]{0:T(128)S(1)}, f32[4]{0:T(128)}, u32[]{:S(2)}) copy-start(f32[4]{0:T(128)} %param.23) | copy-start | bytes 52
  57.0 40.5 %copy-start.9 = (f32[1024]{0:T(1024)S(1)}, f32[1024]{0:T(1024)}, u32[]{:S(2)}) copy-start(f32[1024]{0:T(1024)} %param.26) | copy-start | bytes 12292
  57.7 62.1 %reduce-scatter.3.cloned.1.call-start = ((), (), s32[]{:S(2)}) async-start(), calls=%async_computation.3 | async-start | bytes 122880 | tf_op jit(solution)/shard_map/reduce_scatter | solution.py:106
  94.5 2.9 %copy-start.3 = (f32[24,1024]{1,0:T(8,128)S(1)}, f32[24,1024]{1,0:T(8,128)}, u32[]{:S(2)}) copy-start(f32[24,1024]{1,0:T(8,128)} %get-tuple-element.9) | copy-start | bytes 294916
  94.5 2.9 %copy-start.4 = (f32[24,1024]{1,0:T(8,128)S(1)}, f32[24,1024]{1,0:T(8,128)}, u32[]{:S(2)}) copy-start(f32[24,1024]{1,0:T(8,128)} %get-tuple-element.10) | copy-start | bytes 294916
  94.6 2.9 %copy-start.5 = (f32[24,1024]{1,0:T(8,128)S(1)}, f32[24,1024]{1,0:T(8,128)}, u32[]{:S(2)}) copy-start(f32[24,1024]{1,0:T(8,128)} %get-tuple-element.12) | copy-start | bytes 294916
  96.9 22.9 %copy-start.7 = (bf16[24,256]{1,0:T(8,128)(2,1)S(1)}, bf16[24,256]{1,0:T(8,128)(2,1)}, u32[]{:S(2)}) copy-start(bf16[24,256]{1,0:T(8,128)(2,1)} %param.16) | copy-start | bytes 36868
  96.9 28.8 %copy-start.8 = (f32[1024]{0:T(1024)S(1)}, f32[1024]{0:T(1024)}, u32[]{:S(2)}) copy-start(f32[1024]{0:T(1024)} %param.28) | copy-start | bytes 12292
  100.2 72.9 %all-reduce.8.cloned.1.call-start = ((), (), s32[]{:S(2)}) async-start(), calls=%async_computation.5 | async-start | bytes 1081344 | tf_op jit(solution)/shard_map/psum | solution.py:114
  134.2 63.2 %reduce-scatter.5.cloned.1.call-start = ((), (), s32[]{:S(2)}) async-start(), calls=%async_computation.4 | async-start | bytes 122880 | tf_op jit(solution)/shard_map/reduce_scatter | solution.py:118
Sparse Core Ops, SparseCore 0:
  15.0 36.2 all-reduce.5
  57.8 36.6 all-reduce.9
  100.3 19.4 reduce-scatter.2
  134.3 38.7 all-reduce.7
  177.7 19.6 reduce-scatter.4
where the time goes:
time: 206 us; the launch traced here: 205 us
  waiting for transfers between devices  122 us (59%)
  blocking collectives  36.1 us (18%)
  matrix products  25.7 us (12%)
  between operations  13.4 us (7%)
  other arithmetic  5.31 us (3%)
  local copies, waits for them, and re-layouts  2.77 us (1%)
    psum x1, waiting for transfers between devices, local(): cached = lax.psum(partial_value.reshape(batch_rows, heads_here * DK), 'kv')  36.8 us
    psum x1, waiting for transfers between devices, local(): gate_sum, up_sum = lax.psum((gate_part, up_part), 'kv')  26.8 us
    reduce_scatter x1, waiting for transfers between devices, local(): down = lax.psum_scatter(down_partial, 'tp', scatter_dimension=1, tiled=True)  19.9 us
    reduce_scatter x1, waiting for transfers between devices, local(): mixed = lax.psum_scatter(out_partial, 'tp', scatter_dimension=1, tiled=True)  19.6 us
    psum x1, waiting for transfers between devices, local(): lax.psum((part_query, part_key, part_value, part_gate), 'kv')  18.7 us
    psum x1, blocking collectives, input_stat(): return lax.psum(own_squares, 'kv')  12.4 us
    psum x1, blocking collectives, channel_stat(): return lax.psum(own_squares, 'kv')  11.9 us
    all_gather x1, blocking collectives, local(): row_block = lax.all_gather(tokens, 'tp', axis=1, tiled=True)  6.58 us
  transfers between devices with their start and end apart: 5, of which 5 were waited for; matrix products, arithmetic and copies ran while one was open for 3% of the time, Pallas kernels for 0%

commit v1 on v0

--- a/solution.py
+++ b/solution.py
@@ -1,6 +1,11 @@
+import functools
+import math
+
 import jax
 import jax.numpy as jnp
 from jax import lax
+from jax.experimental import pallas as pl
+from jax.experimental.pallas import tpu as pltpu
 from jax.sharding import PartitionSpec as P
 
 DK = 256
@@ -119,28 +124,514 @@
     return (resid.astype(jnp.float32) + down).astype(jnp.bfloat16)
 
 
+LANES = 128
+F32 = jnp.float32
+BF16 = jnp.bfloat16
+
+
+def window_start(index, tiles, width, parts):
+    return (index * (tiles - width) + (parts - 1) // 2) // (parts - 1)
+
+
+def layer_kernel(
+    n_kv,
+    n_tp,
+    tokens_ref,
+    lengths_ref,
+    attn_gain_ref,
+    log_decay_ref,
+    gn_gain_ref,
+    ffn_gain_ref,
+    wq_hbm,
+    wk_hbm,
+    wv_hbm,
+    wg_hbm,
+    kc_hbm,
+    vc_hbm,
+    wo_hbm,
+    wfg_hbm,
+    wfu_hbm,
+    wfd_hbm,
+    out_ref,
+    wq,
+    wk,
+    wv,
+    wg,
+    kc,
+    vc,
+    wo,
+    wfg,
+    wfu,
+    wfd,
+    tok_buf,
+    x_buf,
+    sq_send,
+    sq_recv,
+    q_send,
+    q_recv,
+    q_full,
+    trig,
+    decay_buf,
+    kvg_send,
+    kvg_recv,
+    cached_buf,
+    ca_send,
+    ca_recv,
+    gt_buf,
+    o_buf,
+    resid_buf,
+    sqm_send,
+    sqm_recv,
+    gu_send,
+    gu_recv,
+    hid_buf,
+    down_buf,
+    d_send,
+    d_recv,
+    load_sem,
+    kv_send_sem,
+    kv_recv_sem,
+    tp_send_sem,
+    tp_recv_sem,
+):
+    rows, own_cols = tokens_ref.shape
+    depth, wide = wq.shape
+    span = kc.shape[1]
+    half = DK // 2
+    tiles = wfg.shape[1] // LANES
+    win = hid_buf.shape[2]
+    me_kv = lax.axis_index("kv")
+    me_tp = lax.axis_index("tp")
+
+    def kv_peer(j):
+        return lax.rem(me_kv + j, n_kv)
+
+    def kv_from(j):
+        return lax.rem(me_kv + n_kv - j, n_kv)
+
+    def tp_peer(j):
+        return lax.rem(me_tp + j, n_tp)
+
+    def tp_from(j):
+        return lax.rem(me_tp + n_tp - j, n_tp)
+
+    loads = {}
+    for slot, (name, src, dst) in enumerate(
+        (
+            ("wq", wq_hbm, wq),
+            ("kc", kc_hbm, kc),
+            ("vc", vc_hbm, vc),
+            ("wk", wk_hbm, wk),
+            ("wv", wv_hbm, wv),
+            ("wg", wg_hbm, wg),
+            ("wo", wo_hbm, wo),
+            ("wfg", wfg_hbm, wfg),
+            ("wfu", wfu_hbm, wfu),
+            ("wfd", wfd_hbm, wfd),
+        )
+    ):
+        loads[name] = pltpu.make_async_copy(src, dst, load_sem.at[slot])
+
+    sent = []
+
+    def to_kv(phase, j, src, dst):
+        copy = pltpu.make_async_remote_copy(
+            src_ref=src,
+            dst_ref=dst,
+            send_sem=kv_send_sem.at[phase, j],
+            recv_sem=kv_recv_sem.at[phase, j],
+            device_id={"kv": kv_peer(j)},
+            device_id_type=pl.DeviceIdType.MESH,
+        )
+        copy.start()
+        sent.append(copy)
+        return copy
+
+    def to_tp(phase, j, src, dst):
+        copy = pltpu.make_async_remote_copy(
+            src_ref=src,
+            dst_ref=dst,
+            send_sem=tp_send_sem.at[phase, j],
+            recv_sem=tp_recv_sem.at[phase, j],
+            device_id={"tp": tp_peer(j)},
+            device_id_type=pl.DeviceIdType.MESH,
+        )
+        copy.start()
+        sent.append(copy)
+        return copy
+
+    loads["wq"].start()
+
+    barrier = pltpu.get_barrier_semaphore()
+    for j in range(1, n_kv):
+        pl.semaphore_signal(
+            barrier, inc=1, device_id={"kv": kv_peer(j)}, device_id_type=pl.DeviceIdType.MESH
+        )
+    for j in range(1, n_tp):
+        pl.semaphore_signal(
+            barrier, inc=1, device_id={"tp": tp_peer(j)}, device_id_type=pl.DeviceIdType.MESH
+        )
+    for name in ("kc", "wk", "wv", "wg", "vc"):
+        loads[name].start()
+    pl.semaphore_wait(barrier, n_kv + n_tp - 2)
+
+    tok_copies = [to_tp(0, j, tokens_ref, tok_buf.at[me_tp]) for j in range(1, n_tp)]
+    tok_buf[me_tp] = tokens_ref[...]
+
+    row_id = lax.broadcasted_iota(jnp.int32, (rows, LANES), 0)
+    lens = jnp.zeros((rows, LANES), jnp.int32)
+    for b in range(rows):
+        lens = jnp.where(row_id == b, lengths_ref[b], lens)
+    lane = lax.broadcasted_iota(jnp.int32, (rows, half), 1).astype(F32)
+    inverse = jnp.exp(lane * (-math.log(ROPE_BASE) / half))
+    angles = lens[:, :1].astype(F32) * inverse
+    trig[0] = jnp.cos(angles)
+    trig[1] = jnp.sin(angles)
+    places = rows * span
+    col = lax.broadcasted_iota(jnp.int32, (rows, places), 1)
+    row = lax.broadcasted_iota(jnp.int32, (rows, places), 0)
+    slot = col - row * span
+    position = slot + me_kv * span
+    gap = lens[:, :1] - position
+    live = (slot >= 0) & (slot < span) & (gap > 0)
+    gap_f = jnp.where(live, gap, 0).astype(F32)
+    for h in range(n_kv):
+        decay_buf[h] = jnp.where(live, jnp.exp(gap_f * log_decay_ref[h]), 0.0)
+
+    def rotate_in(front, back):
+        cosine, sine = trig[0], trig[1]
+        return front * cosine - back * sine, front * sine + back * cosine
+
+    for copy in tok_copies:
+        copy.wait_recv()
+    squares = jnp.zeros((rows, 1), F32)
+    for c in range(n_tp):
+        wide_tok = tok_buf[c].astype(F32)
+        squares = squares + jnp.sum(wide_tok * wide_tok, axis=1, keepdims=True)
+        cols = pl.ds(c * own_cols, own_cols)
+        x_buf[:, cols] = (wide_tok * attn_gain_ref[:, cols]).astype(BF16)
+    sq_send[...] = jnp.broadcast_to(squares, (rows, LANES))
+    sq_copies = [to_kv(0, j, sq_send, sq_recv.at[j]) for j in range(1, n_kv)]
+
+    x = x_buf[...]
+    loads["wq"].wait()
+    q_own = jnp.dot(x, wq[...], preferred_element_type=F32)
+    q_send[...] = q_own.astype(BF16)
+    q_full[...] = q_own
+    q_copies = [to_kv(1, j, q_send, q_recv.at[j]) for j in range(1, n_kv)]
+    for name in ("wo", "wfg", "wfu", "wfd"):
+        loads[name].start()
+
+    for name in ("wk", "wv", "wg"):
+        loads[name].wait()
+    kvg_copies = []
+    own_kvg = []
+    for j in tuple(range(1, n_kv)) + (0,):
+        cols = pl.ds(pl.multiple_of(kv_peer(j) * DK, DK), DK)
+        for i, weight in enumerate((wk, wv, wg)):
+            part = jnp.dot(x, weight[:, cols], preferred_element_type=F32)
+            if j:
+                kvg_send[j, :, pl.ds(i * DK, DK)] = part.astype(BF16)
+            else:
+                own_kvg.append(part)
+        if j:
+            kvg_copies.append(to_kv(2, j, kvg_send.at[j], kvg_recv.at[j]))
+
+    for copy in sq_copies:
+        copy.wait_recv()
+    total_sq = sq_send[...]
+    for j in range(1, n_kv):
+        total_sq = total_sq + sq_recv[j]
+    factor = lax.rsqrt(total_sq / D + RMS_EPS)[:, :1]
+
+    for copy in q_copies:
+        copy.wait_recv()
+    loads["kc"].wait()
+    loads["vc"].wait()
+    for h in range(n_kv):
+        halves = []
+        for lo in (h * DK, h * DK + half):
+            cols = pl.ds(lo, half)
+            piece = q_full[:, cols]
+            for j in range(1, n_kv):
+                piece = piece + q_recv[j, :, cols].astype(F32)
+            halves.append(piece * factor)
+        front, back = rotate_in(*halves)
+        q_full[:, pl.ds(h * DK, half)] = front * DK ** (-0.5)
+        q_full[:, pl.ds(h * DK + half, half)] = back * DK ** (-0.5)
+        cols = pl.ds(h * DK, DK)
+        keys = kc[:, :, cols].reshape(places, DK)
+        scores = lax.dot_general(
+            q_full[:, cols].astype(BF16),
+            keys,
+            (((1,), (1,)), ((), ())),
+            preferred_element_type=F32,
+        )
+        mixing = (scores * decay_buf[h]).astype(BF16)
+        values = vc[:, :, cols].reshape(places, DK)
+        cached_buf[:, cols] = jnp.dot(mixing, values, preferred_element_type=F32)
+    ca_copies = []
+    for j in range(1, n_kv):
+        cols = pl.ds(pl.multiple_of(kv_peer(j) * DK, DK), DK)
+        ca_send[j] = cached_buf[:, cols].astype(BF16)
+        ca_copies.append(to_kv(3, j, ca_send.at[j], ca_recv.at[j]))
+
+    for copy in kvg_copies:
+        copy.wait_recv()
+    own_head = pl.ds(pl.multiple_of(me_kv * DK, DK), DK)
+    summed = []
+    for i in range(3):
+        piece = own_kvg[i]
+        for j in range(1, n_kv):
+            piece = piece + kvg_recv[j, :, pl.ds(i * DK, DK)].astype(F32)
+        summed.append(piece * factor)
+    new_key, new_value, gate = summed
+    front, back = rotate_in(new_key[:, :half], new_key[:, half:])
+    query = q_full[:, own_head]
+    score = jnp.sum(query[:, :half] * front + query[:, half:] * back, axis=1, keepdims=True)
+    own_term = score * new_value
+    gate = gate / (1.0 + jnp.exp(-gate))
+    totals = own_term + cached_buf[:, own_head]
+    for copy in ca_copies:
+        copy.wait_recv()
+    for j in range(1, n_kv):
+        totals = totals + ca_recv[j].astype(F32)
+    center = jnp.sum(totals, axis=1, keepdims=True) / DK
+    spread = jnp.sum(totals * totals, axis=1, keepdims=True) / DK - center * center
+    normed = (totals - center) * lax.rsqrt(spread + GN_EPS) * gn_gain_ref[:, own_head]
+    gt_buf[me_kv] = (gate * normed).astype(BF16)
+    gt_copies = [to_kv(4, j, gt_buf.at[me_kv], gt_buf.at[me_kv]) for j in range(1, n_kv)]
+
+    loads["wo"].wait()
+    for copy in gt_copies:
+        copy.wait_recv()
+    for c in range(n_kv):
+        x_buf[:, pl.ds(c * DK, DK)] = gt_buf[c]
+    o_buf[me_tp] = jnp.dot(x_buf[...], wo[...], preferred_element_type=F32).astype(BF16)
+    o_copies = [to_tp(1, j, o_buf.at[me_tp], o_buf.at[me_tp]) for j in range(1, n_tp)]
+    for copy in o_copies:
+        copy.wait_recv()
+    squares = jnp.zeros((rows, 1), F32)
+    for c in range(n_tp):
+        cols = pl.ds(c * own_cols, own_cols)
+        mixed = o_buf[0, :, cols].astype(F32)
+        for t in range(1, n_tp):
+            mixed = mixed + o_buf[t, :, cols].astype(F32)
+        resid = (tok_buf[c].astype(F32) + mixed).astype(BF16)
+        resid_wide = resid.astype(F32)
+        resid_buf[c] = resid_wide
+        squares = squares + jnp.sum(resid_wide * resid_wide, axis=1, keepdims=True)
+        x_buf[:, cols] = (resid_wide * ffn_gain_ref[:, cols]).astype(BF16)
+    sqm_send[...] = jnp.broadcast_to(squares, (rows, LANES))
+    sqm_copies = [to_kv(5, j, sqm_send, sqm_recv.at[j]) for j in range(1, n_kv)]
+
+    x = x_buf[...]
+    loads["wfg"].wait()
+    loads["wfu"].wait()
+    gu_copies = []
+    own_gu = []
+    for j in tuple(range(1, n_kv)) + (0,):
+        start = window_start(kv_peer(j), tiles, win // LANES, n_kv)
+        cols = pl.ds(pl.multiple_of(start * LANES, LANES), win)
+        for i, weight in enumerate((wfg, wfu)):
+            part = jnp.dot(x, weight[:, cols], preferred_element_type=F32)
+            if j:
+                gu_send[j, :, pl.ds(i * win, win)] = part.astype(BF16)
+            else:
+                own_gu.append(part)
+        if j:
+            gu_copies.append(to_kv(6, j, gu_send.at[j], gu_recv.at[j]))
+
+    for copy in sqm_copies:
+        copy.wait_recv()
+    total_sq = sqm_send[...]
+    for j in range(1, n_kv):
+        total_sq = total_sq + sqm_recv[j]
+    factor = lax.rsqrt(total_sq / D + RMS_EPS)[:, :1]
+    for copy in gu_copies:
+        copy.wait_recv()
+    summed = []
+    for i in range(2):
+        piece = own_gu[i]
+        for j in range(1, n_kv):
+            piece = piece + gu_recv[j, :, pl.ds(i * win, win)].astype(F32)
+        summed.append(piece * factor)
+    gate, up = summed
+    hidden = gate / (1.0 + jnp.exp(-gate)) * up
+    here = window_start(me_kv, tiles, win // LANES, n_kv)
+    after = window_start(me_kv + 1, tiles, win // LANES, n_kv)
+    kept = jnp.where(me_kv == n_kv - 1, win, (after - here) * LANES)
+    column = lax.broadcasted_iota(jnp.int32, (rows, win), 1)
+    hid_buf[me_kv] = jnp.where(column < kept, hidden, 0.0).astype(BF16)
+    hid_copies = [to_kv(7, j, hid_buf.at[me_kv], hid_buf.at[me_kv]) for j in range(1, n_kv)]
+
+    loads["wfd"].wait()
+    down = None
+    for j in range(n_kv):
+        if j:
+            hid_copies[j - 1].wait_recv()
+        source = kv_from(j)
+        start = window_start(source, tiles, win // LANES, n_kv)
+        weight = wfd[pl.ds(pl.multiple_of(start * LANES, LANES), win), :]
+        part = jnp.dot(hid_buf[source], weight, preferred_element_type=F32)
+        down = part if down is None else down + part
+    down_buf[...] = down
+    d_copies = []
+    for j in range(1, n_tp):
+        cols = pl.ds(pl.multiple_of(tp_peer(j) * own_cols, own_cols), own_cols)
+        d_send[j] = down_buf[:, cols].astype(BF16)
+        d_copies.append(to_tp(2, j, d_send.at[j], d_recv.at[j]))
+    own = pl.ds(pl.multiple_of(me_tp * own_cols, own_cols), own_cols)
+    result = down_buf[:, own] + resid_buf[me_tp]
+    for j in range(1, n_tp):
+        d_copies[j - 1].wait_recv()
+        result = result + d_recv[j].astype(F32)
+    out_ref[...] = result.astype(BF16)
+    for copy in sent:
+        copy.wait_send()
+
+
+def fused(
+    n_kv,
+    n_tp,
+    tokens,
+    lengths,
+    attn_gain,
+    w_query,
+    w_key,
+    w_value,
+    w_gate,
+    log_decay,
+    key_cache,
+    value_cache,
+    gn_gain,
+    w_out,
+    ffn_gain,
+    w_ffn_gate,
+    w_ffn_up,
+    w_ffn_down,
+):
+    rows, own_cols = tokens.shape
+    depth, wide = w_query.shape
+    units = w_ffn_gate.shape[1]
+    tiles = units // LANES
+    win = -(-tiles // n_kv) * LANES
+    span = key_cache.shape[1]
+    vmem = pl.BlockSpec(memory_space=pltpu.VMEM)
+    smem = pl.BlockSpec(memory_space=pltpu.SMEM)
+    hbm = pl.BlockSpec(memory_space=pl.ANY)
+    streamed = (
+        w_query,
+        w_key,
+        w_value,
+        w_gate,
+        key_cache,
+        value_cache,
+        w_out,
+        w_ffn_gate,
+        w_ffn_up,
+        w_ffn_down,
+    )
+    scratch = [pltpu.VMEM(a.shape, a.dtype) for a in streamed] + [
+        pltpu.VMEM((n_tp, rows, own_cols), BF16),
+        pltpu.VMEM((rows, depth), BF16),
+        pltpu.VMEM((rows, LANES), F32),
+        pltpu.VMEM((n_kv, rows, LANES), F32),
+        pltpu.VMEM((rows, wide), BF16),
+        pltpu.VMEM((n_kv, rows, wide), BF16),
+        pltpu.VMEM((rows, wide), F32),
+        pltpu.VMEM((2, rows, DK // 2), F32),
+        pltpu.VMEM((n_kv, rows, rows * span), F32),
+        pltpu.VMEM((n_kv, rows, 3 * DK), BF16),
+        pltpu.VMEM((n_kv, rows, 3 * DK), BF16),
+        pltpu.VMEM((rows, wide), F32),
+        pltpu.VMEM((n_kv, rows, DK), BF16),
+        pltpu.VMEM((n_kv, rows, DK), BF16),
+        pltpu.VMEM((n_kv, rows, DK), BF16),
+        pltpu.VMEM((n_tp, rows, depth), BF16),
+        pltpu.VMEM((n_tp, rows, own_cols), F32),
+        pltpu.VMEM((rows, LANES), F32),
+        pltpu.VMEM((n_kv, rows, LANES), F32),
+        pltpu.VMEM((n_kv, rows, 2 * win), BF16),
+        pltpu.VMEM((n_kv, rows, 2 * win), BF16),
+        pltpu.VMEM((n_kv, rows, win), BF16),
+        pltpu.VMEM((rows, depth), F32),
+        pltpu.VMEM((n_tp, rows, own_cols), BF16),
+        pltpu.VMEM((n_tp, rows, own_cols), BF16),
+        pltpu.SemaphoreType.DMA((len(streamed),)),
+        pltpu.SemaphoreType.DMA((8, n_kv)),
+        pltpu.SemaphoreType.DMA((8, n_kv)),
+        pltpu.SemaphoreType.DMA((3, n_tp)),
+        pltpu.SemaphoreType.DMA((3, n_tp)),
+    ]
+    return pl.pallas_call(
+        functools.partial(layer_kernel, n_kv, n_tp),
+        out_shape=jax.ShapeDtypeStruct((rows, own_cols), BF16),
+        in_specs=[vmem, smem, vmem, smem, vmem, vmem] + [hbm] * len(streamed),
+        out_specs=vmem,
+        scratch_shapes=scratch,
+        compiler_params=pltpu.CompilerParams(
+            collective_id=0, has_side_effects=True, vmem_limit_bytes=60 * 1024 * 1024
+        ),
+    )(
+        tokens,
+        lengths,
+        attn_gain[None, :],
+        log_decay,
+        gn_gain[None, :],
+        ffn_gain[None, :],
+        *streamed,
+    )
+
+
+def fits(mesh, tokens, log_decay, key_cache, w_query, w_ffn_gate):
+    n_kv, n_tp, n_grp = mesh.shape["kv"], mesh.shape["tp"], mesh.shape["grp"]
+    heads, span = log_decay.shape[0], key_cache.shape[1] // n_kv
+    return (
+        n_kv > 1
+        and n_tp > 1
+        and heads == n_kv * n_tp
+        and tokens.shape[1] // n_kv == heads * DK // n_tp
+        and tokens.shape[1] % (n_kv * n_tp * LANES) == 0
+        and w_ffn_gate.shape[1] % (n_tp * LANES) == 0
+        and tokens.shape[0] // n_grp % 8 == 0
+        and span % 16 == 0
+        and span <= 64
+    )
+
+
 def solution(mesh):
-    return jax.shard_map(
-        local,
-        mesh=mesh,
-        in_specs=(
-            P("grp", ("kv", "tp")),
-            P("grp"),
-            P("kv"),
-            P("kv", "tp"),
-            P("kv", "tp"),
-            P("kv", "tp"),
-            P("kv", "tp"),
-            P("tp"),
-            P("grp", "kv", "tp"),
-            P("grp", "kv", "tp"),
-            P("tp"),
-            P("tp", "kv"),
-            P("kv"),
-            P("kv", "tp"),
-            P("kv", "tp"),
-            P("tp", "kv"),
-        ),
-        out_specs=P("grp", ("kv", "tp")),
-        check_vma=False,
+    specs = (
+        P("grp", ("kv", "tp")),
+        P("grp"),
+        P("kv"),
+        P("kv", "tp"),
+        P("kv", "tp"),
+        P("kv", "tp"),
+        P("kv", "tp"),
+        P("tp"),
+        P("grp", "kv", "tp"),
+        P("grp", "kv", "tp"),
+        P("tp"),
+        P("tp", "kv"),
+        P("kv"),
+        P("kv", "tp"),
+        P("kv", "tp"),
+        P("tp", "kv"),
     )
+
+    def whole(*arrays):
+        tokens, w_query, log_decay, key_cache = arrays[0], arrays[3], arrays[7], arrays[8]
+        if fits(mesh, tokens, log_decay, key_cache, w_query, arrays[13]):
+            body = functools.partial(fused, mesh.shape["kv"], mesh.shape["tp"])
+        else:
+            body = local
+        return jax.shard_map(
+            body,
+            mesh=mesh,
+            in_specs=specs,
+            out_specs=P("grp", ("kv", "tp")),
+            check_vma=False,
+        )(*arrays)
+
+    return whole

time: 206 us -> 51.7 us (0.25)
  waiting for transfers between devices: 122 us -> 0 us
  Pallas kernels: 0 us -> 50.1 us
  blocking collectives: 36.1 us -> 0 us
  matrix products: 25.7 us -> 0 us
  between operations: 13.4 us -> 0.01 us
  other arithmetic: 5.31 us -> 0 us
    psum x3 -> x0, waiting for transfers between devices: 82.3 us -> none  [the longest x1 36.8 us: local(): cached = lax.psum(partial_value.reshape(batch_rows, heads_here * DK), 'kv')]
    pallas_call x0 -> x1, Pallas kernels: none -> 50.1 us  [fused(): pl.pallas_call(functools.partial(layer_kernel, n_kv, n_tp), out_shape=jax...]
    reduce_scatter x2 -> x0, waiting for transfers between devices: 39.4 us -> none  [the longest x1 19.9 us: local(): down = lax.psum_scatter(down_partial, 'tp', scatter_dimension=1, tiled=True)]
    dot_general x10 -> x0, matrix products: 25.7 us -> none  [the longest x1 4.39 us: local(): jnp.dot(hidden, w_ffn_down, preferred_element_type=jnp.float32)]
    psum x2 -> x0, blocking collectives: 24.3 us -> none  [the longest x1 12.4 us: input_stat(): return lax.psum(own_squares, 'kv')]
    all_gather x2 -> x0, blocking collectives: 11.8 us -> none  [the longest x1 6.58 us: local(): row_block = lax.all_gather(tokens, 'tp', axis=1, tiled=True)]
    convert_element_type x5 -> x0, other arithmetic: 2.39 us -> none  [the longest x1 1.34 us: local(): return (resid.astype(jnp.float32) + down).astype(jnp.bfloat16)]
  transfers between devices with their start and end apart: 5 -> 0, of which waited for: 5 -> 0; matrix products, arithmetic and copies ran while one was open for 3% -> 0% of each run, Pallas kernels for 0% -> 0%
where the time goes in v1:
time: 51.7 us; the launch traced here: 51.4 us
  Pallas kernels  50.1 us (97%)
  local copies, waits for them, and re-layouts  1.31 us (3%)
    pallas_call x1, Pallas kernels, fused(): pl.pallas_call(functools.partial(layer_kernel, n_kv, n_tp), out_shape=jax...  50.1 us
    unnamed x1, local copies, waits for them, and re-layouts  1.31 us

profile of v1, /device:TPU:0, one launch (start us, length us, event | category | flops | bytes accessed | tf_op | source)
XLA Modules:
  0.0 51.4 jit_solution(15857479154062473894)
XLA Ops:
  0.0 50.1 %shard_map.154 = bf16[24,256]{1,0:T(8,128)(2,1)} custom-call(bf16[24,256]{1,0:T(8,128)(2,1)} %tokens_ref.1, s32[24]{0:T(128)} %lengths_ref.1, f32[1,1024]{1,0:T(1,128)} %bitcast.3, f32[4]{0:T(128)} %log_decay_ref.1, f32[1,1024]{1,0:T(1,128)} %bitcast.4, f32[1,1024]{1,0:T(1,128)} %bitcast.5, bf16[1024,1024]{1,0:T(8,128)(2,1)} %wq_hbm.1, ...), custom_call_target="tpu_custom_call" | custom-call | tf_op jit(solution)/shard_map/pallas_call | solution.py:567
  50.1 1.3 %copy.18 = bf16[24,256]{1,0:T(8,128)(2,1)} copy(bf16[24,256]{1,0:T(8,128)(2,1)} %shard_map.154) | data formatting | bytes 24576

commit v2 on v1

--- a/solution.py
+++ b/solution.py
@@ -131,6 +131,26 @@
 
 def window_start(index, tiles, width, parts):
     return (index * (tiles - width) + (parts - 1) // 2) // (parts - 1)
+
+
+def partner(index, j, parts):
+    found, bit = 0, 1
+    while bit < parts:
+        digit = (index // bit) % 2
+        found = found + bit * ((1 - digit) if (j // bit) % 2 else digit)
+        bit *= 2
+    return found
+
+
+def pack(value):
+    middle = value.shape[1] // 2
+    return jnp.concatenate([value[:, :middle], value[:, middle:]], axis=0).astype(BF16)
+
+
+def unpack(packed):
+    wide = packed.astype(F32)
+    rows = wide.shape[0] // 2
+    return jnp.concatenate([wide[:rows], wide[rows:]], axis=1)
 
 
 def layer_kernel(
@@ -199,21 +219,18 @@
     span = kc.shape[1]
     half = DK // 2
     tiles = wfg.shape[1] // LANES
-    win = hid_buf.shape[2]
+    win = gu_send.shape[2]
     me_kv = lax.axis_index("kv")
     me_tp = lax.axis_index("tp")
 
     def kv_peer(j):
-        return lax.rem(me_kv + j, n_kv)
-
-    def kv_from(j):
-        return lax.rem(me_kv + n_kv - j, n_kv)
+        return partner(me_kv, j, n_kv)
 
     def tp_peer(j):
-        return lax.rem(me_tp + j, n_tp)
-
-    def tp_from(j):
-        return lax.rem(me_tp + n_tp - j, n_tp)
+        return partner(me_tp, j, n_tp)
+
+    kv_order = tuple(range(n_kv - 1, 0, -1))
+    tp_order = tuple(range(n_tp - 1, 0, -1))
 
     loads = {}
     for slot, (name, src, dst) in enumerate(
@@ -271,11 +288,11 @@
         pl.semaphore_signal(
             barrier, inc=1, device_id={"tp": tp_peer(j)}, device_id_type=pl.DeviceIdType.MESH
         )
-    for name in ("kc", "wk", "wv", "wg", "vc"):
+    pl.semaphore_wait(barrier, n_kv + n_tp - 2)
+
+    tok_copies = [to_tp(0, j, tokens_ref, tok_buf.at[me_tp]) for j in tp_order]
+    for name in ("wk", "wv", "wg", "kc", "vc"):
         loads[name].start()
-    pl.semaphore_wait(barrier, n_kv + n_tp - 2)
-
-    tok_copies = [to_tp(0, j, tokens_ref, tok_buf.at[me_tp]) for j in range(1, n_tp)]
     tok_buf[me_tp] = tokens_ref[...]
 
     row_id = lax.broadcasted_iota(jnp.int32, (rows, LANES), 0)
@@ -311,31 +328,30 @@
         cols = pl.ds(c * own_cols, own_cols)
         x_buf[:, cols] = (wide_tok * attn_gain_ref[:, cols]).astype(BF16)
     sq_send[...] = jnp.broadcast_to(squares, (rows, LANES))
-    sq_copies = [to_kv(0, j, sq_send, sq_recv.at[j]) for j in range(1, n_kv)]
+    sq_copies = [to_kv(0, j, sq_send, sq_recv.at[j]) for j in kv_order]
 
     x = x_buf[...]
     loads["wq"].wait()
     q_own = jnp.dot(x, wq[...], preferred_element_type=F32)
-    q_send[...] = q_own.astype(BF16)
+    q_send[...] = pack(q_own)
     q_full[...] = q_own
-    q_copies = [to_kv(1, j, q_send, q_recv.at[j]) for j in range(1, n_kv)]
+    q_copies = [to_kv(1, j, q_send, q_recv.at[j]) for j in kv_order]
     for name in ("wo", "wfg", "wfu", "wfd"):
         loads[name].start()
 
     for name in ("wk", "wv", "wg"):
         loads[name].wait()
     kvg_copies = []
-    own_kvg = []
-    for j in tuple(range(1, n_kv)) + (0,):
+    for j in kv_order + (0,):
         cols = pl.ds(pl.multiple_of(kv_peer(j) * DK, DK), DK)
-        for i, weight in enumerate((wk, wv, wg)):
-            part = jnp.dot(x, weight[:, cols], preferred_element_type=F32)
-            if j:
-                kvg_send[j, :, pl.ds(i * DK, DK)] = part.astype(BF16)
-            else:
-                own_kvg.append(part)
+        parts = [
+            jnp.dot(x, weight[:, cols], preferred_element_type=F32) for weight in (wk, wv, wg)
+        ]
         if j:
+            kvg_send[j] = pack(jnp.concatenate(parts, axis=1))
             kvg_copies.append(to_kv(2, j, kvg_send.at[j], kvg_recv.at[j]))
+        else:
+            own_kvg = jnp.concatenate(parts, axis=1)
 
     for copy in sq_copies:
         copy.wait_recv()
@@ -348,14 +364,12 @@
         copy.wait_recv()
     loads["kc"].wait()
     loads["vc"].wait()
+    query = q_full[...]
+    for j in kv_order:
+        query = query + unpack(q_recv[j])
+    query = query * factor
     for h in range(n_kv):
-        halves = []
-        for lo in (h * DK, h * DK + half):
-            cols = pl.ds(lo, half)
-            piece = q_full[:, cols]
-            for j in range(1, n_kv):
-                piece = piece + q_recv[j, :, cols].astype(F32)
-            halves.append(piece * factor)
+        halves = (query[:, h * DK : h * DK + half], query[:, h * DK + half : (h + 1) * DK])
         front, back = rotate_in(*halves)
         q_full[:, pl.ds(h * DK, half)] = front * DK ** (-0.5)
         q_full[:, pl.ds(h * DK + half, half)] = back * DK ** (-0.5)
@@ -371,20 +385,18 @@
         values = vc[:, :, cols].reshape(places, DK)
         cached_buf[:, cols] = jnp.dot(mixing, values, preferred_element_type=F32)
     ca_copies = []
-    for j in range(1, n_kv):
+    for j in kv_order:
         cols = pl.ds(pl.multiple_of(kv_peer(j) * DK, DK), DK)
-        ca_send[j] = cached_buf[:, cols].astype(BF16)
+        ca_send[j] = pack(cached_buf[:, cols])
         ca_copies.append(to_kv(3, j, ca_send.at[j], ca_recv.at[j]))
 
     for copy in kvg_copies:
         copy.wait_recv()
     own_head = pl.ds(pl.multiple_of(me_kv * DK, DK), DK)
-    summed = []
-    for i in range(3):
-        piece = own_kvg[i]
-        for j in range(1, n_kv):
-            piece = piece + kvg_recv[j, :, pl.ds(i * DK, DK)].astype(F32)
-        summed.append(piece * factor)
+    for j in kv_order:
+        own_kvg = own_kvg + unpack(kvg_recv[j])
+    own_kvg = own_kvg * factor
+    summed = [own_kvg[:, i * DK : (i + 1) * DK] for i in range(3)]
     new_key, new_value, gate = summed
     front, back = rotate_in(new_key[:, :half], new_key[:, half:])
     query = q_full[:, own_head]
@@ -395,51 +407,49 @@
     for copy in ca_copies:
         copy.wait_recv()
     for j in range(1, n_kv):
-        totals = totals + ca_recv[j].astype(F32)
+        totals = totals + unpack(ca_recv[j])
     center = jnp.sum(totals, axis=1, keepdims=True) / DK
     spread = jnp.sum(totals * totals, axis=1, keepdims=True) / DK - center * center
     normed = (totals - center) * lax.rsqrt(spread + GN_EPS) * gn_gain_ref[:, own_head]
-    gt_buf[me_kv] = (gate * normed).astype(BF16)
-    gt_copies = [to_kv(4, j, gt_buf.at[me_kv], gt_buf.at[me_kv]) for j in range(1, n_kv)]
+    gt_buf[me_kv] = pack(gate * normed)
+    gt_copies = [to_kv(4, j, gt_buf.at[me_kv], gt_buf.at[me_kv]) for j in kv_order]
 
     loads["wo"].wait()
     for copy in gt_copies:
         copy.wait_recv()
     for c in range(n_kv):
-        x_buf[:, pl.ds(c * DK, DK)] = gt_buf[c]
-    o_buf[me_tp] = jnp.dot(x_buf[...], wo[...], preferred_element_type=F32).astype(BF16)
-    o_copies = [to_tp(1, j, o_buf.at[me_tp], o_buf.at[me_tp]) for j in range(1, n_tp)]
+        x_buf[:, pl.ds(c * DK, DK)] = unpack(gt_buf[c]).astype(BF16)
+    o_buf[me_tp] = pack(jnp.dot(x_buf[...], wo[...], preferred_element_type=F32))
+    o_copies = [to_tp(1, j, o_buf.at[me_tp], o_buf.at[me_tp]) for j in tp_order]
     for copy in o_copies:
         copy.wait_recv()
     squares = jnp.zeros((rows, 1), F32)
+    mixed = unpack(o_buf[0])
+    for t in range(1, n_tp):
+        mixed = mixed + unpack(o_buf[t])
     for c in range(n_tp):
         cols = pl.ds(c * own_cols, own_cols)
-        mixed = o_buf[0, :, cols].astype(F32)
-        for t in range(1, n_tp):
-            mixed = mixed + o_buf[t, :, cols].astype(F32)
-        resid = (tok_buf[c].astype(F32) + mixed).astype(BF16)
+        own_mixed = mixed[:, c * own_cols : (c + 1) * own_cols]
+        resid = (tok_buf[c].astype(F32) + own_mixed).astype(BF16)
         resid_wide = resid.astype(F32)
         resid_buf[c] = resid_wide
         squares = squares + jnp.sum(resid_wide * resid_wide, axis=1, keepdims=True)
         x_buf[:, cols] = (resid_wide * ffn_gain_ref[:, cols]).astype(BF16)
     sqm_send[...] = jnp.broadcast_to(squares, (rows, LANES))
-    sqm_copies = [to_kv(5, j, sqm_send, sqm_recv.at[j]) for j in range(1, n_kv)]
+    sqm_copies = [to_kv(5, j, sqm_send, sqm_recv.at[j]) for j in kv_order]
 
     x = x_buf[...]
     loads["wfg"].wait()
     loads["wfu"].wait()
     gu_copies = []
-    own_gu = []
-    for j in tuple(range(1, n_kv)) + (0,):
+    for j in kv_order + (0,):
         start = window_start(kv_peer(j), tiles, win // LANES, n_kv)
         cols = pl.ds(pl.multiple_of(start * LANES, LANES), win)
-        for i, weight in enumerate((wfg, wfu)):
-            part = jnp.dot(x, weight[:, cols], preferred_element_type=F32)
-            if j:
-                gu_send[j, :, pl.ds(i * win, win)] = part.astype(BF16)
-            else:
-                own_gu.append(part)
+        gate = jnp.dot(x, wfg[:, cols], preferred_element_type=F32)
+        up = jnp.dot(x, wfu[:, cols], preferred_element_type=F32)
+        both = jnp.concatenate([gate, up], axis=0)
         if j:
+            gu_send[j] = both.astype(BF16)
             gu_copies.append(to_kv(6, j, gu_send.at[j], gu_recv.at[j]))
 
     for copy in sqm_copies:
@@ -450,42 +460,40 @@
     factor = lax.rsqrt(total_sq / D + RMS_EPS)[:, :1]
     for copy in gu_copies:
         copy.wait_recv()
-    summed = []
-    for i in range(2):
-        piece = own_gu[i]
-        for j in range(1, n_kv):
-            piece = piece + gu_recv[j, :, pl.ds(i * win, win)].astype(F32)
-        summed.append(piece * factor)
-    gate, up = summed
+    for j in kv_order:
+        both = both + gu_recv[j].astype(F32)
+    gate, up = both[:rows] * factor, both[rows:] * factor
     hidden = gate / (1.0 + jnp.exp(-gate)) * up
     here = window_start(me_kv, tiles, win // LANES, n_kv)
     after = window_start(me_kv + 1, tiles, win // LANES, n_kv)
     kept = jnp.where(me_kv == n_kv - 1, win, (after - here) * LANES)
     column = lax.broadcasted_iota(jnp.int32, (rows, win), 1)
-    hid_buf[me_kv] = jnp.where(column < kept, hidden, 0.0).astype(BF16)
-    hid_copies = [to_kv(7, j, hid_buf.at[me_kv], hid_buf.at[me_kv]) for j in range(1, n_kv)]
+    hid_buf[me_kv] = pack(jnp.where(column < kept, hidden, 0.0))
+    hid_copies = [to_kv(7, j, hid_buf.at[me_kv], hid_buf.at[me_kv]) for j in kv_order]
 
     loads["wfd"].wait()
     down = None
+    arrivals = dict(zip(kv_order, hid_copies))
     for j in range(n_kv):
         if j:
-            hid_copies[j - 1].wait_recv()
-        source = kv_from(j)
+            arrivals[j].wait_recv()
+        source = kv_peer(j)
         start = window_start(source, tiles, win // LANES, n_kv)
         weight = wfd[pl.ds(pl.multiple_of(start * LANES, LANES), win), :]
-        part = jnp.dot(hid_buf[source], weight, preferred_element_type=F32)
+        chunk = unpack(hid_buf[source]).astype(BF16)
+        part = jnp.dot(chunk, weight, preferred_element_type=F32)
         down = part if down is None else down + part
     down_buf[...] = down
-    d_copies = []
-    for j in range(1, n_tp):
+    d_copies = {}
+    for j in tp_order:
         cols = pl.ds(pl.multiple_of(tp_peer(j) * own_cols, own_cols), own_cols)
-        d_send[j] = down_buf[:, cols].astype(BF16)
-        d_copies.append(to_tp(2, j, d_send.at[j], d_recv.at[j]))
+        d_send[j] = pack(down_buf[:, cols])
+        d_copies[j] = to_tp(2, j, d_send.at[j], d_recv.at[j])
     own = pl.ds(pl.multiple_of(me_tp * own_cols, own_cols), own_cols)
     result = down_buf[:, own] + resid_buf[me_tp]
     for j in range(1, n_tp):
-        d_copies[j - 1].wait_recv()
-        result = result + d_recv[j].astype(F32)
+        d_copies[j].wait_recv()
+        result = result + unpack(d_recv[j])
     out_ref[...] = result.astype(BF16)
     for copy in sent:
         copy.wait_send()
@@ -515,7 +523,7 @@
     depth, wide = w_query.shape
     units = w_ffn_gate.shape[1]
     tiles = units // LANES
-    win = -(-tiles // n_kv) * LANES
+    win = -(-tiles // n_kv // 2) * 2 * LANES
     span = key_cache.shape[1]
     vmem = pl.BlockSpec(memory_space=pltpu.VMEM)
     smem = pl.BlockSpec(memory_space=pltpu.SMEM)
@@ -537,27 +545,27 @@
         pltpu.VMEM((rows, depth), BF16),
         pltpu.VMEM((rows, LANES), F32),
         pltpu.VMEM((n_kv, rows, LANES), F32),
-        pltpu.VMEM((rows, wide), BF16),
-        pltpu.VMEM((n_kv, rows, wide), BF16),
+        pltpu.VMEM((2 * rows, wide // 2), BF16),
+        pltpu.VMEM((n_kv, 2 * rows, wide // 2), BF16),
         pltpu.VMEM((rows, wide), F32),
         pltpu.VMEM((2, rows, DK // 2), F32),
         pltpu.VMEM((n_kv, rows, rows * span), F32),
-        pltpu.VMEM((n_kv, rows, 3 * DK), BF16),
-        pltpu.VMEM((n_kv, rows, 3 * DK), BF16),
+        pltpu.VMEM((n_kv, 2 * rows, 3 * DK // 2), BF16),
+        pltpu.VMEM((n_kv, 2 * rows, 3 * DK // 2), BF16),
         pltpu.VMEM((rows, wide), F32),
-        pltpu.VMEM((n_kv, rows, DK), BF16),
-        pltpu.VMEM((n_kv, rows, DK), BF16),
-        pltpu.VMEM((n_kv, rows, DK), BF16),
-        pltpu.VMEM((n_tp, rows, depth), BF16),
+        pltpu.VMEM((n_kv, 2 * rows, DK // 2), BF16),
+        pltpu.VMEM((n_kv, 2 * rows, DK // 2), BF16),
+        pltpu.VMEM((n_kv, 2 * rows, DK // 2), BF16),
+        pltpu.VMEM((n_tp, 2 * rows, depth // 2), BF16),
         pltpu.VMEM((n_tp, rows, own_cols), F32),
         pltpu.VMEM((rows, LANES), F32),
         pltpu.VMEM((n_kv, rows, LANES), F32),
-        pltpu.VMEM((n_kv, rows, 2 * win), BF16),
-        pltpu.VMEM((n_kv, rows, 2 * win), BF16),
-        pltpu.VMEM((n_kv, rows, win), BF16),
+        pltpu.VMEM((n_kv, 2 * rows, win), BF16),
+        pltpu.VMEM((n_kv, 2 * rows, win), BF16),
+        pltpu.VMEM((n_kv, 2 * rows, win // 2), BF16),
         pltpu.VMEM((rows, depth), F32),
-        pltpu.VMEM((n_tp, rows, own_cols), BF16),
-        pltpu.VMEM((n_tp, rows, own_cols), BF16),
+        pltpu.VMEM((n_tp, 2 * rows, own_cols // 2), BF16),
+        pltpu.VMEM((n_tp, 2 * rows, own_cols // 2), BF16),
         pltpu.SemaphoreType.DMA((len(streamed),)),
         pltpu.SemaphoreType.DMA((8, n_kv)),
         pltpu.SemaphoreType.DMA((8, n_kv)),
@@ -590,9 +598,11 @@
     return (
         n_kv > 1
         and n_tp > 1
+        and n_kv & (n_kv - 1) == 0
+        and n_tp & (n_tp - 1) == 0
         and heads == n_kv * n_tp
         and tokens.shape[1] // n_kv == heads * DK // n_tp
-        and tokens.shape[1] % (n_kv * n_tp * LANES) == 0
+        and tokens.shape[1] % (n_kv * n_tp * 2 * LANES) == 0
         and w_ffn_gate.shape[1] % (n_tp * LANES) == 0
         and tokens.shape[0] // n_grp % 8 == 0
         and span % 16 == 0

time: 51.7 us -> 50.2 us (0.971)
  Pallas kernels: 50.1 us -> 48.7 us
    pallas_call x1, Pallas kernels: 50.1 us -> 48.7 us  [fused(): pl.pallas_call(functools.partial(layer_kernel, n_kv, n_tp), out_shape=jax...]
where the time goes in v2:
time: 50.2 us; the launch traced here: 50 us
  Pallas kernels  48.7 us (97%)
  local copies, waits for them, and re-layouts  1.31 us (3%)
    pallas_call x1, Pallas kernels, fused(): pl.pallas_call(functools.partial(layer_kernel, n_kv, n_tp), out_shape=jax...  48.7 us
    unnamed x1, local copies, waits for them, and re-layouts  1.31 us

profile of v2, /device:TPU:0, one launch (start us, length us, event | category | flops | bytes accessed | tf_op | source)
XLA Modules:
  0.0 50.0 jit_solution(5439749418416307399)
XLA Ops:
  0.0 48.7 %shard_map.154 = bf16[24,256]{1,0:T(8,128)(2,1)} custom-call(bf16[24,256]{1,0:T(8,128)(2,1)} %tokens_ref.1, s32[24]{0:T(128)} %lengths_ref.1, f32[1,1024]{1,0:T(1,128)} %bitcast.3, f32[4]{0:T(128)} %log_decay_ref.1, f32[1,1024]{1,0:T(1,128)} %bitcast.4, f32[1,1024]{1,0:T(1,128)} %bitcast.5, bf16[1024,1024]{1,0:T(8,128)(2,1)} %wq_hbm.1, ...), custom_call_target="tpu_custom_call" | custom-call | tf_op jit(solution)/shard_map/pallas_call | solution.py:575
  48.7 1.3 %copy.18 = bf16[24,256]{1,0:T(8,128)(2,1)} copy(bf16[24,256]{1,0:T(8,128)(2,1)} %shard_map.154) | data formatting | bytes 24576

commit v3 on v2

--- a/solution.py
+++ b/solution.py
@@ -194,7 +194,6 @@
     decay_buf,
     kvg_send,
     kvg_recv,
-    cached_buf,
     ca_send,
     ca_recv,
     gt_buf,
@@ -219,7 +218,7 @@
     span = kc.shape[1]
     half = DK // 2
     tiles = wfg.shape[1] // LANES
-    win = gu_send.shape[2]
+    win = gu_send.shape[3] * 2
     me_kv = lax.axis_index("kv")
     me_tp = lax.axis_index("tp")
 
@@ -332,10 +331,14 @@
 
     x = x_buf[...]
     loads["wq"].wait()
-    q_own = jnp.dot(x, wq[...], preferred_element_type=F32)
-    q_send[...] = pack(q_own)
-    q_full[...] = q_own
-    q_copies = [to_kv(1, j, q_send, q_recv.at[j]) for j in kv_order]
+    q_copies = []
+    for part in range(2):
+        cols = pl.ds(part * (wide // 2), wide // 2)
+        q_own = jnp.dot(x, wq[:, cols], preferred_element_type=F32)
+        q_send[part] = pack(q_own)
+        q_full[:, cols] = q_own
+        for j in kv_order:
+            q_copies.append(to_kv(1 + 7 * part, j, q_send.at[part], q_recv.at[part, j]))
     for name in ("wo", "wfg", "wfu", "wfd"):
         loads[name].start()
 
@@ -360,20 +363,26 @@
         total_sq = total_sq + sq_recv[j]
     factor = lax.rsqrt(total_sq / D + RMS_EPS)[:, :1]
 
-    for copy in q_copies:
-        copy.wait_recv()
     loads["kc"].wait()
     loads["vc"].wait()
-    query = q_full[...]
-    for j in kv_order:
-        query = query + unpack(q_recv[j])
-    query = query * factor
+    for copy in q_copies:
+        copy.wait_recv()
+    parts = []
+    for part in range(2):
+        piece = q_full[:, pl.ds(part * (wide // 2), wide // 2)]
+        for j in kv_order:
+            piece = piece + unpack(q_recv[part, j])
+        parts.append(piece * factor)
+    query = jnp.concatenate(parts, axis=1)
     for h in range(n_kv):
         halves = (query[:, h * DK : h * DK + half], query[:, h * DK + half : (h + 1) * DK])
         front, back = rotate_in(*halves)
         q_full[:, pl.ds(h * DK, half)] = front * DK ** (-0.5)
         q_full[:, pl.ds(h * DK + half, half)] = back * DK ** (-0.5)
-        cols = pl.ds(h * DK, DK)
+    ca_copies = []
+    for j in kv_order + (0,):
+        head = kv_peer(j)
+        cols = pl.ds(pl.multiple_of(head * DK, DK), DK)
         keys = kc[:, :, cols].reshape(places, DK)
         scores = lax.dot_general(
             q_full[:, cols].astype(BF16),
@@ -381,14 +390,12 @@
             (((1,), (1,)), ((), ())),
             preferred_element_type=F32,
         )
-        mixing = (scores * decay_buf[h]).astype(BF16)
+        mixing = (scores * decay_buf[head]).astype(BF16)
         values = vc[:, :, cols].reshape(places, DK)
-        cached_buf[:, cols] = jnp.dot(mixing, values, preferred_element_type=F32)
-    ca_copies = []
-    for j in kv_order:
-        cols = pl.ds(pl.multiple_of(kv_peer(j) * DK, DK), DK)
-        ca_send[j] = pack(cached_buf[:, cols])
-        ca_copies.append(to_kv(3, j, ca_send.at[j], ca_recv.at[j]))
+        cached = jnp.dot(mixing, values, preferred_element_type=F32)
+        if j:
+            ca_send[j] = pack(cached)
+            ca_copies.append(to_kv(3, j, ca_send.at[j], ca_recv.at[j]))
 
     for copy in kvg_copies:
         copy.wait_recv()
@@ -403,7 +410,7 @@
     score = jnp.sum(query[:, :half] * front + query[:, half:] * back, axis=1, keepdims=True)
     own_term = score * new_value
     gate = gate / (1.0 + jnp.exp(-gate))
-    totals = own_term + cached_buf[:, own_head]
+    totals = own_term + cached
     for copy in ca_copies:
         copy.wait_recv()
     for j in range(1, n_kv):
@@ -445,12 +452,13 @@
     for j in kv_order + (0,):
         start = window_start(kv_peer(j), tiles, win // LANES, n_kv)
         cols = pl.ds(pl.multiple_of(start * LANES, LANES), win)
-        gate = jnp.dot(x, wfg[:, cols], preferred_element_type=F32)
-        up = jnp.dot(x, wfu[:, cols], preferred_element_type=F32)
-        both = jnp.concatenate([gate, up], axis=0)
-        if j:
-            gu_send[j] = both.astype(BF16)
-            gu_copies.append(to_kv(6, j, gu_send.at[j], gu_recv.at[j]))
+        both = []
+        for i, weight in enumerate((wfg, wfu)):
+            part = jnp.dot(x, weight[:, cols], preferred_element_type=F32)
+            both.append(part)
+            if j:
+                gu_send[i, j] = pack(part)
+                gu_copies.append(to_kv(6 + 3 * i, j, gu_send.at[i, j], gu_recv.at[i, j]))
 
     for copy in sqm_copies:
         copy.wait_recv()
@@ -460,9 +468,10 @@
     factor = lax.rsqrt(total_sq / D + RMS_EPS)[:, :1]
     for copy in gu_copies:
         copy.wait_recv()
-    for j in kv_order:
-        both = both + gu_recv[j].astype(F32)
-    gate, up = both[:rows] * factor, both[rows:] * factor
+    for i in range(2):
+        for j in kv_order:
+            both[i] = both[i] + unpack(gu_recv[i, j])
+    gate, up = both[0] * factor, both[1] * factor
     hidden = gate / (1.0 + jnp.exp(-gate)) * up
     here = window_start(me_kv, tiles, win // LANES, n_kv)
     after = window_start(me_kv + 1, tiles, win // LANES, n_kv)
@@ -545,14 +554,13 @@
         pltpu.VMEM((rows, depth), BF16),
         pltpu.VMEM((rows, LANES), F32),
         pltpu.VMEM((n_kv, rows, LANES), F32),
-        pltpu.VMEM((2 * rows, wide // 2), BF16),
-        pltpu.VMEM((n_kv, 2 * rows, wide // 2), BF16),
+        pltpu.VMEM((2, 2 * rows, wide // 4), BF16),
+        pltpu.VMEM((2, n_kv, 2 * rows, wide // 4), BF16),
         pltpu.VMEM((rows, wide), F32),
         pltpu.VMEM((2, rows, DK // 2), F32),
         pltpu.VMEM((n_kv, rows, rows * span), F32),
         pltpu.VMEM((n_kv, 2 * rows, 3 * DK // 2), BF16),
         pltpu.VMEM((n_kv, 2 * rows, 3 * DK // 2), BF16),
-        pltpu.VMEM((rows, wide), F32),
         pltpu.VMEM((n_kv, 2 * rows, DK // 2), BF16),
         pltpu.VMEM((n_kv, 2 * rows, DK // 2), BF16),
         pltpu.VMEM((n_kv, 2 * rows, DK // 2), BF16),
@@ -560,21 +568,21 @@
         pltpu.VMEM((n_tp, rows, own_cols), F32),
         pltpu.VMEM((rows, LANES), F32),
         pltpu.VMEM((n_kv, rows, LANES), F32),
-        pltpu.VMEM((n_kv, 2 * rows, win), BF16),
-        pltpu.VMEM((n_kv, 2 * rows, win), BF16),
+        pltpu.VMEM((2, n_kv, 2 * rows, win // 2), BF16),
+        pltpu.VMEM((2, n_kv, 2 * rows, win // 2), BF16),
         pltpu.VMEM((n_kv, 2 * rows, win // 2), BF16),
         pltpu.VMEM((rows, depth), F32),
         pltpu.VMEM((n_tp, 2 * rows, own_cols // 2), BF16),
         pltpu.VMEM((n_tp, 2 * rows, own_cols // 2), BF16),
         pltpu.SemaphoreType.DMA((len(streamed),)),
-        pltpu.SemaphoreType.DMA((8, n_kv)),
-        pltpu.SemaphoreType.DMA((8, n_kv)),
+        pltpu.SemaphoreType.DMA((10, n_kv)),
+        pltpu.SemaphoreType.DMA((10, n_kv)),
         pltpu.SemaphoreType.DMA((3, n_tp)),
         pltpu.SemaphoreType.DMA((3, n_tp)),
     ]
     return pl.pallas_call(
         functools.partial(layer_kernel, n_kv, n_tp),
-        out_shape=jax.ShapeDtypeStruct((rows, own_cols), BF16),
+        out_shape=pltpu.VMEM((rows, own_cols), BF16),
         in_specs=[vmem, smem, vmem, smem, vmem, vmem] + [hbm] * len(streamed),
         out_specs=vmem,
         scratch_shapes=scratch,
@@ -603,6 +611,7 @@
         and heads == n_kv * n_tp
         and tokens.shape[1] // n_kv == heads * DK // n_tp
         and tokens.shape[1] % (n_kv * n_tp * 2 * LANES) == 0
+        and heads * DK // n_tp % (4 * LANES) == 0
         and w_ffn_gate.shape[1] % (n_tp * LANES) == 0
         and tokens.shape[0] // n_grp % 8 == 0
         and span % 16 == 0

time: 50.2 us -> 48.8 us (0.972)
  local copies, waits for them, and re-layouts: 1.31 us -> 0.6 us
  Pallas kernels: 48.7 us -> 48 us
    unnamed x1, local copies, waits for them, and re-layouts: 1.31 us -> 0.6 us
    pallas_call x1, Pallas kernels: 48.7 us -> 48 us  [fused(): pl.pallas_call(functools.partial(layer_kernel, n_kv, n_tp), out_shape=plt...]
where the time goes in v3:
time: 48.8 us; the launch traced here: 48.6 us
  Pallas kernels  48 us (98%)
  local copies, waits for them, and re-layouts  0.6 us (1%)
    pallas_call x1, Pallas kernels, fused(): pl.pallas_call(functools.partial(layer_kernel, n_kv, n_tp), out_shape=plt...  48 us

profile of v3, /device:TPU:0, one launch (start us, length us, event | category | flops | bytes accessed | tf_op | source)
XLA Modules:
  0.0 48.6 jit_solution(8630044649731392750)
XLA Ops:
  0.0 48.0 %shard_map.154 = bf16[24,256]{1,0:T(8,128)(2,1)S(1)} custom-call(bf16[24,256]{1,0:T(8,128)(2,1)} %tokens_ref.1, s32[24]{0:T(128)} %lengths_ref.1, f32[1,1024]{1,0:T(1,128)} %bitcast.3, f32[4]{0:T(128)} %log_decay_ref.1, f32[1,1024]{1,0:T(1,128)} %bitcast.4, f32[1,1024]{1,0:T(1,128)} %bitcast.5, bf16[1024,1024]{1,0:T(8,128)(2,1)} %wq_hbm.1, ...), custom_call_target="tpu_custom_call" | custom-call | tf_op jit(solution)/shard_map/pallas_call | solution.py:583
  48.0 0.6 %copy.18 = bf16[24,256]{1,0:T(8,128)(2,1)} copy(bf16[24,256]{1,0:T(8,128)(2,1)S(1)} %shard_map.154) | data formatting | bytes 24576
